TPU v7x, 32 devices: a whole 2x2x4 slice. The times are simulated.
32 devices in a mesh: grp: 2 (over y), dp: 2 (over x), kv: 4 (over z), tp: 2 (over core).
Axes of the slice: x: 2, y: 2, z: 4, core: 2. Of those that a mesh axis runs over, the one named last changes fastest.
Arguments:
- queries: bfloat16 [4, 1024, 2048], P(('grp', 'dp'), 'kv', 'tp'), parts along dimension 0, may hold values from -10 to 10
- keys: bfloat16 [4, 1024, 512], P(('grp', 'dp'), 'kv', 'tp'), parts along dimension 0, may hold values from -10 to 10
- values: bfloat16 [4, 1024, 512], P(('grp', 'dp'), 'kv', 'tp'), parts along dimension 0, may hold values from -6 to 6
- gate_logits: float32 [4, 2, 1024, 32], P(('grp', 'dp'), None, 'kv', 'tp'), parts along dimension 0, may hold values from -6 to 6
- chosen: int32 [4, 8, 8, 16], P(('grp', 'dp'), 'kv', 'tp'), parts along dimension 0, may hold values from -1 to 15, as said below
- pool_k: float32 [32, 64], replicated, may hold values from 0 to 0.35
- pool_v: float32 [32, 64], replicated, may hold values from 0 to 0.35
- out_gain: float32 [2048], P('tp'), may hold values from 0.1 to 1.9
Outputs:
- attended: bfloat16 [4, 1024, 2048], P(('grp', 'dp'), 'kv', 'tp'), parts along dimension 0
There are 2 independent parts, one for each index of `grp`. A program takes and returns all parts, laid end to end along the dimension named above; an argument that names none is the same for every part. Nothing has to cross between parts.
Inputs may be any that keep to these rules, and one draw needn't show every extreme that they name: Entries are key block numbers (block e holds positions e * 64 to e * 64 + 63) or -1 for none. The list of query block b (positions b * 128 onward) holds the blocks that contain its own positions, other distinct blocks that begin before it, and -1 in its remaining entries. For the query blocks of one span of 256 positions and one key head, the blocks chosen from any other span number at most 2; in every draw some span reaches 2.
All inputs are finite; a program needn't handle non-finite values.
Results may differ from a plain program's by a relative error of at most 0.0079.
Values may be sent and summed in bfloat16 or wider, within the bound.
A program may use at most 64 MiB of HBM per device.

v0:
```python
import functools

import jax
import jax.numpy as jnp
from jax import lax
from jax.experimental import pallas as pl
from jax.experimental.pallas import tpu as pltpu
from jax.sharding import PartitionSpec as P

DH = 64
CMP_STRIDE = 16
CMP_BLOCK = 32
SLC = 64
QB = 128
MOST = 2
THETA = 500000.0
EPS = 1e-06
NEG = -1e30
LOG2E = 1.4426950408889634
MESH = pl.DeviceIdType.MESH


def rope_table(start, length):
    half = DH // 2
    lane = jnp.arange(2 * DH)
    freq = jnp.power(jnp.float32(THETA), -(2.0 * (lane % half).astype(jnp.float32)) / DH)
    angle = (start + jnp.arange(length)).astype(jnp.float32)[:, None] * freq[None, :]
    sign = jnp.where(lane % DH < half, -1.0, 1.0).astype(jnp.float32)
    return jnp.cos(angle), jnp.sin(angle) * sign[None, :]


def turn(x, cosine, sine):
    half = DH // 2
    lane = lax.broadcasted_iota(jnp.int32, x.shape, 1)
    partner = jnp.where(lane % DH < half, pltpu.roll(x, 2 * DH - half, 1), pltpu.roll(x, half, 1))
    return (x * cosine + partner * sine).astype(jnp.bfloat16)


def kernel(
    n, q_ref, k_ref, v_ref, gate_ref, list_ref, pk_ref, pv_ref, gain_ref, cos_ref, sin_ref,
    out_ref,
    qt, kt, vtl, kk, kkr, vtr, skk, svt, req, reqbuf, flag, own_bias, far_bias,
    sumbuf, edge, sendk, sendv, recvk, recvv, bias,
    top, total, acc, stot, sacc,
    req_send, req_recv, sum_send, sum_recv, edge_send, edge_recv,
    k_send, k_recv, v_send, v_recv,
):
    me = lax.axis_index("kv")
    length = q_ref.shape[1]
    heads = q_ref.shape[2] // DH
    groups = k_ref.shape[2] // DH
    per_group = heads // groups
    pairs = per_group // 2
    slabs = groups // 2
    qblocks = length // QB
    per = length // SLC
    count = length // CMP_STRIDE
    scale = DH ** (-0.5) * LOG2E
    f32 = jnp.float32

    barrier = pltpu.get_barrier_semaphore()
    for d in range(1, n):
        pl.semaphore_signal(
            barrier, inc=1, device_id={"kv": lax.rem(me + d, n)}, device_id_type=MESH
        )

    lanes = req.shape[1]
    rows = qblocks * groups

    def column(x, at):
        spot = lax.broadcasted_iota(jnp.int32, x.shape, 1) == at
        picked = jnp.sum(jnp.where(spot, x.astype(f32), 0.0), 1, keepdims=True)
        return jnp.broadcast_to(picked, (x.shape[0], QB))

    lists = jnp.concatenate([list_ref[0, b] for b in range(qblocks)], 0)
    lane = lax.broadcasted_iota(jnp.int32, (rows, lanes), 1)
    member = jnp.zeros((rows, lanes), jnp.int32)
    for i in range(lists.shape[1]):
        member = jnp.where(lists[:, i : i + 1] == lane, 1, member)
    union = member[:groups]
    for b in range(1, qblocks):
        union = jnp.maximum(union, member[b * groups : (b + 1) * groups])
    union = jnp.concatenate([union] * qblocks, 0)
    inner = lane % per
    rank = jnp.zeros_like(union)
    for d in range(1, per):
        rank = rank + jnp.where(inner >= d, pltpu.roll(union, d, 1), 0)

    def first_of(x):
        found = x
        for d in range(1, per):
            found = found + pltpu.roll(x, lanes - d, 1)
        return found

    for j in range(MOST):
        hit = (union == 1) & (rank == j)
        asked = first_of(jnp.where(hit, inner, 0))
        req[j * groups : (j + 1) * groups, :] = asked[:groups]
        flag[j * rows : (j + 1) * rows, :] = first_of(jnp.where(hit, member, 0))
    for i in range(per):
        own_bias[i] = jnp.where(column(member, me * per + i) > 0.5, 0.0, NEG)

    pl.semaphore_wait(barrier, n - 1)

    def remote(src, dst, send, recv, peer, origin):
        return pltpu.make_async_remote_copy(
            src_ref=src, dst_ref=dst, send_sem=send.at[peer], recv_sem=recv.at[origin],
            device_id={"kv": peer}, device_id_type=MESH,
        )

    def ask(peer, origin):
        return remote(req, reqbuf.at[origin], req_send, req_recv, peer, origin)

    def give_sum(peer, origin):
        return remote(sumbuf.at[origin], sumbuf.at[origin], sum_send, sum_recv, peer, origin)

    def give_edge(peer, origin):
        return remote(edge.at[origin], edge.at[origin], edge_send, edge_recv, peer, origin)

    def give_k(peer, origin):
        return remote(sendk.at[peer], recvk.at[origin], k_send, k_recv, peer, origin)

    def give_v(peer, origin):
        return remote(sendv.at[peer], recvv.at[origin], v_send, v_recv, peer, origin)

    @pl.loop(0, me)
    def _(d):
        ask(me - 1 - d, me).start()

    cosine = cos_ref[...]
    sine = sin_ref[...]
    low = lax.broadcasted_iota(jnp.int32, (length, 2 * DH), 1) < DH
    for p in range(slabs):
        cols = slice(p * 2 * DH, (p + 1) * 2 * DH)
        turned = turn(k_ref[0, :, cols].astype(f32), cosine, sine)
        kt[:, cols] = turned
    row = lax.broadcasted_iota(jnp.int32, (count, 2 * DH), 0)
    for w, (src, pool_ref) in enumerate(((k_ref, pk_ref), (v_ref, pv_ref))):
        pool = pool_ref[...]
        pool = jnp.concatenate([pool, pool], 1)
        for p in range(slabs):
            cols = slice(p * 2 * DH, (p + 1) * 2 * DH)
            x = src[0, :, cols].astype(f32).reshape(count, CMP_STRIDE, 2 * DH)
            lower = jnp.sum(x * pool[None, :CMP_STRIDE], 1)
            upper = jnp.sum(x * pool[None, CMP_STRIDE:], 1)
            following = jnp.where(row == count - 1, 0.0, pltpu.roll(upper, count - 1, 0))
            sumbuf[me, w, :, cols] = (lower + following).astype(jnp.bfloat16)
            edge[me, 2 * w : 2 * w + 1, cols] = lower[count - 1 :]
            edge[me, 2 * w + 1 : 2 * w + 2, cols] = upper[:1]

    @pl.loop(me + 1, n)
    def _(r):
        give_sum(r, me).start()
        give_edge(r, me).start()

    low_slc = lax.broadcasted_iota(jnp.int32, (SLC, 2 * DH), 1) < DH

    odd = lax.rem(me, 2)

    @pl.loop(0, n - 1 - me)
    def _(d):
        r = odd * (me + 1 + d) + (1 - odd) * (n - 1 - d)
        ask(me, r).wait_recv()
        ids = column(reqbuf[r], me * per)
        for j in range(MOST):
            place = slice(j * SLC, (j + 1) * SLC)
            for p in range(slabs):
                cols = slice(p * 2 * DH, (p + 1) * 2 * DH)
                at = j * groups + 2 * p
                pick = jnp.where(low_slc, ids[at : at + 1], ids[at + 1 : at + 2])
                k_block = kt[:SLC, cols].astype(f32)
                v_block = v_ref[0, :SLC, cols].astype(f32)
                for i in range(1, per):
                    span = slice(i * SLC, (i + 1) * SLC)
                    match = pick > i - 0.5
                    k_block = jnp.where(match, kt[span, cols].astype(f32), k_block)
                    v_block = jnp.where(match, v_ref[0, span, cols].astype(f32), v_block)
                sendk[r, place, cols] = k_block.astype(jnp.bfloat16)
                sendv[r, place, cols] = v_block.astype(jnp.bfloat16)
        give_k(r, me).start()
        give_v(r, me).start()

    for p in range(heads // 2):
        qt[p] = turn(q_ref[0, :, p * 2 * DH : (p + 1) * 2 * DH].astype(f32), cosine, sine)

    def spread(slab, g, dst):
        keep = lax.broadcasted_iota(jnp.int32, slab.shape, 1) < DH
        wide = slab.astype(f32)
        swapped = pltpu.roll(wide, DH, 1)
        first, second = (wide, swapped) if g % 2 == 0 else (swapped, wide)
        dst[g, 0] = jnp.where(keep, first, 0.0).astype(jnp.bfloat16)
        dst[g, 1] = jnp.where(keep, 0.0, second).astype(jnp.bfloat16)

    def transposed(slab):
        return slab.astype(f32).T.astype(jnp.bfloat16)

    def score(keys, queries):
        return lax.dot_general(
            keys, queries, (((1,), (1,)), ((), ())), preferred_element_type=f32
        )

    for g in range(groups):
        spread(kt[:, (g // 2) * 2 * DH : (g // 2 + 1) * 2 * DH], g, kk)
    for p in range(slabs):
        flip = transposed(v_ref[0, :, p * 2 * DH : (p + 1) * 2 * DH])
        vtl[2 * p] = flip[:DH]
        vtl[2 * p + 1] = flip[DH:]
    key_at = lax.broadcasted_iota(jnp.int32, (SLC, QB), 0)
    token_at = lax.broadcasted_iota(jnp.int32, (SLC, QB), 1)

    @pl.loop(0, groups, unroll=2)
    def _(g):
        for b in range(qblocks):
            for i in range(per):
                value = own_bias[i, pl.ds(b * groups + g, 1), :]
                tile = jnp.where(key_at + i * SLC <= token_at + b * QB, value, NEG)
                bias[i * SLC : (i + 1) * SLC, b * QB : (b + 1) * QB] = tile
        both = kk[g].reshape(2 * length, 2 * DH)
        allowed = bias[...]
        raw = [score(both, qt[g * pairs + pair]) * scale for pair in range(pairs)]
        parts = [
            r[e * length : (e + 1) * length] + allowed for r in raw for e in range(2)
        ]
        tops = [jnp.max(x, 0, keepdims=True) for x in parts]
        weights = [jnp.exp2(x - m) for x, m in zip(parts, tops)]
        totals = [jnp.sum(w, 0, keepdims=True) for w in weights]
        flat = vtl[g]
        sums = [
            jnp.dot(flat, w.astype(jnp.bfloat16), preferred_element_type=f32) for w in weights
        ]
        for o in range(per_group):
            h = g * per_group + o
            top[h] = tops[o]
            total[h] = totals[o]
            acc[h] = sums[o]

    @pl.loop(0, me)
    def _(d):
        give_sum(me, me - 1 - d).wait_recv()
        give_edge(me, me - 1 - d).wait_recv()

    for s in range(n):
        for w in range(2):
            place = slice(s * count, (s + 1) * count)
            for p in range(slabs):
                cols = slice(p * 2 * DH, (p + 1) * 2 * DH)
                following = edge[min(s + 1, n - 1), 2 * w + 1 : 2 * w + 2, cols]
                last = edge[s, 2 * w : 2 * w + 1, cols] + following
                own = sumbuf[s, w, :, cols].astype(f32)
                joined = jnp.where((row == count - 1) & (s < me), last, own)
                joined = jnp.where(s <= me, joined, 0.0)
                if w == 0:
                    for o in range(2):
                        lanes_low = lax.broadcasted_iota(jnp.int32, joined.shape, 1) < DH
                        swapped = pltpu.roll(joined, DH, 1)
                        first, second = (joined, swapped) if o == 0 else (swapped, joined)
                        skk[2 * p + o, 0, place] = jnp.where(lanes_low, first, 0.0).astype(
                            jnp.bfloat16
                        )
                        skk[2 * p + o, 1, place] = jnp.where(lanes_low, 0.0, second).astype(
                            jnp.bfloat16
                        )
                else:
                    svt[place, cols] = joined.astype(jnp.bfloat16)
    part_at = lax.broadcasted_iota(jnp.int32, (n * count, length), 0)
    time_at = lax.broadcasted_iota(jnp.int32, (n * count, length), 1) + me * length
    seen = part_at * CMP_STRIDE + CMP_BLOCK - 1 <= time_at
    sbias = jnp.where(seen, 0.0, NEG)
    flips = [transposed(svt[:, p * 2 * DH : (p + 1) * 2 * DH]) for p in range(slabs)]
    for g in range(groups):
        vt = flips[g // 2][(g % 2) * DH : (g % 2 + 1) * DH]
        both = skk[g].reshape(2 * n * count, 2 * DH)
        raw = [
            score(both, q_ref[0, :, (g * pairs + pair) * 2 * DH : (g * pairs + pair + 1) * 2 * DH])
            * scale
            for pair in range(pairs)
        ]
        parts = [
            r[e * n * count : (e + 1) * n * count] + sbias for r in raw for e in range(2)
        ]
        tops = [jnp.maximum(jnp.max(x, 0, keepdims=True), 0.1 * NEG) for x in parts]
        weights = [jnp.exp2(x - m) for x, m in zip(parts, tops)]
        totals = [jnp.sum(w, 0, keepdims=True) for w in weights]
        sums = [jnp.dot(vt, w.astype(jnp.bfloat16), preferred_element_type=f32) for w in weights]
        for o in range(per_group):
            stot[g * per_group + o] = totals[o]
            sacc[g * per_group + o] = sums[o]

    @pl.loop(0, me)
    def _(d):
        s = lax.rem(me - 1 + d, me)
        give_k(me, s).wait_recv()
        give_v(me, s).wait_recv()
        far_bias[...] = jnp.where(column(flag[...], s * per) > 0.5, 0.0, NEG)
        for g in range(groups):
            spread(recvk[s, :, (g // 2) * 2 * DH : (g // 2 + 1) * 2 * DH], g, kkr)
        for p in range(slabs):
            flip = transposed(recvv[s, :, p * 2 * DH : (p + 1) * 2 * DH])
            vtr[2 * p] = flip[:DH]
            vtr[2 * p + 1] = flip[DH:]

        @pl.loop(0, groups, unroll=4)
        def _(g):
            rowed = [
                jnp.concatenate(
                    [
                        far_bias[pl.ds((j * qblocks + b) * groups + g, 1), :]
                        for b in range(qblocks)
                    ],
                    1,
                )
                for j in range(MOST)
            ]
            size = MOST * SLC
            both = kkr[g].reshape(2 * size, 2 * DH)
            base = g * per_group
            old = [top[base + o] for o in range(per_group)]
            old_total = [total[base + o] for o in range(per_group)]
            old_acc = [acc[base + o] for o in range(per_group)]
            raw = [score(both, qt[g * pairs + pair]) * scale for pair in range(pairs)]
            parts = [
                jnp.concatenate(
                    [
                        r[e * size + j * SLC : e * size + (j + 1) * SLC] + rowed[j]
                        for j in range(MOST)
                    ],
                    0,
                )
                for r in raw
                for e in range(2)
            ]
            tops = [jnp.maximum(jnp.max(x, 0, keepdims=True), m) for x, m in zip(parts, old)]
            weights = [jnp.exp2(x - m) for x, m in zip(parts, tops)]
            shrink = [jnp.exp2(a - m) for a, m in zip(old, tops)]
            totals = [
                t * c + jnp.sum(w, 0, keepdims=True)
                for t, c, w in zip(old_total, shrink, weights)
            ]
            flat = vtr[g]
            sums = [
                a * c + jnp.dot(flat, w.astype(jnp.bfloat16), preferred_element_type=f32)
                for a, c, w in zip(old_acc, shrink, weights)
            ]
            for o in range(per_group):
                top[base + o] = tops[o]
                total[base + o] = totals[o]
                acc[base + o] = sums[o]

    for pair in range(heads // 2):
        both = []
        for e in range(2):
            h = 2 * pair + e
            first, second = (
                1.0 / (1.0 + jnp.exp(-gate_ref[0, w, h : h + 1])) for w in range(2)
            )
            mixed = sacc[h] * (first / jnp.maximum(stot[h], 1.0)) + acc[h] * (
                second / total[h]
            )
            mean = jnp.sum(mixed * mixed, 0, keepdims=True) * (1.0 / DH)
            both.append(mixed * lax.rsqrt(mean + EPS))
        cols = slice(pair * 2 * DH, (pair + 1) * 2 * DH)
        flat = jnp.concatenate(both, 0).T
        out_ref[0, :, cols] = (flat * gain_ref[:, cols]).astype(jnp.bfloat16)

    @pl.loop(0, me)
    def _(d):
        ask(me - 1 - d, me).wait_send()

    @pl.loop(me + 1, n)
    def _(r):
        give_sum(r, me).wait_send()
        give_edge(r, me).wait_send()
        give_k(r, me).wait_send()
        give_v(r, me).wait_send()


def per_device(queries, keys, values, gate_logits, chosen, pool_k, pool_v, out_gain):
    n = lax.axis_size("kv")
    length = queries.shape[1]
    groups = keys.shape[2] // DH
    heads = queries.shape[2] // DH
    qblocks = length // QB
    count = length // CMP_STRIDE
    total = n * (length // SLC)
    lanes = -(-total // 128) * 128
    rows = qblocks * groups
    width = groups * DH
    cosine, sine = rope_table(lax.axis_index("kv") * length, length)
    gates = gate_logits.transpose(0, 1, 3, 2)
    bf16, f32, i32 = jnp.bfloat16, jnp.float32, jnp.int32
    vm, dma = pltpu.VMEM, pltpu.SemaphoreType.DMA
    scratch = [
        vm((heads // 2, length, 2 * DH), bf16),
        vm((length, width), bf16),
        vm((groups, DH, length), bf16),
        vm((groups, 2, length, 2 * DH), bf16),
        vm((groups, 2, MOST * SLC, 2 * DH), bf16),
        vm((groups, DH, MOST * SLC), bf16),
        vm((groups, 2, n * count, 2 * DH), bf16),
        vm((n * count, width), bf16),
        vm((MOST * groups, lanes), i32),
        vm((n, MOST * groups, lanes), i32),
        vm((MOST * rows, lanes), i32),
        vm((length // SLC, rows, QB), f32),
        vm((MOST * rows, QB), f32),
        vm((n, 2, count, width), bf16),
        vm((n, 8, width), f32),
        vm((n, MOST * SLC, width), bf16),
        vm((n, MOST * SLC, width), bf16),
        vm((n, MOST * SLC, width), bf16),
        vm((n, MOST * SLC, width), bf16),
        vm((length, length), f32),
        vm((heads, 1, length), f32),
        vm((heads, 1, length), f32),
        vm((heads, DH, length), f32),
        vm((heads, 1, length), f32),
        vm((heads, DH, length), f32),
        dma((n,)), dma((n,)), dma((n,)), dma((n,)), dma((n,)), dma((n,)),
        dma((n,)), dma((n,)), dma((n,)), dma((n,)),
    ]
    return pl.pallas_call(
        functools.partial(kernel, n),
        out_shape=jax.ShapeDtypeStruct(queries.shape, bf16),
        in_specs=[pl.BlockSpec(memory_space=pltpu.VMEM)] * 10,
        out_specs=pl.BlockSpec(memory_space=pltpu.VMEM),
        scratch_shapes=scratch,
        compiler_params=pltpu.CompilerParams(
            collective_id=0, has_side_effects=True, vmem_limit_bytes=48 << 20
        ),
    )(queries, keys, values, gates, chosen, pool_k, pool_v, out_gain[None], cosine, sine)


def solution(mesh):
    in_specs = (
        P(("grp", "dp"), "kv", "tp"),
        P(("grp", "dp"), "kv", "tp"),
        P(("grp", "dp"), "kv", "tp"),
        P(("grp", "dp"), None, "kv", "tp"),
        P(("grp", "dp"), "kv", "tp", None),
        P(),
        P(),
        P("tp"),
    )
    out_specs = P(("grp", "dp"), "kv", "tp")
    return jax.shard_map(
        per_device, mesh=mesh, in_specs=in_specs, out_specs=out_specs, check_vma=False
    )
```

profile of v0, /device:TPU:24, one launch (start us, length us, event | category | flops | bytes accessed | tf_op | source)
XLA Modules:
  0.0 24.2 jit_solution(11240543915239513242)
XLA Ops:
  0.0 0.0 copy-start.7
  0.0 0.0 copy-start.6
  0.0 0.0 copy-start.4
  0.0 0.0 copy-start.1
  0.0 0.0 copy-start.2
  0.1 0.5 %fusion = (f32[256,128]{1,0:T(8,128)S(1)}, f32[256,128]{1,0:T(8,128)S(1)}) fusion(f32[128]{0:T(128)S(1)} %get-tuple-element.7, f32[128]{0:T(128)S(1)} %get-tuple-element.8, f32[256]{0:T(256)S(1)} %add_convert_fusion), kind=kLoop, calls=%fused_computation.2 | loop fusion | flops 65536 | bytes 264192 | tf_op jit(solution)/shard_map/mul | solution.py:29
  0.6 0.1 copy-done.7
  0.7 0.0 copy-done.6
  0.7 0.0 copy-done.4
  0.8 0.2 copy-done.1
  1.0 0.1 copy-done.2
  1.0 0.0 copy-start
  1.0 1.0 %copy-done = bf16[1,256,1024]{2,1,0:T(8,128)(2,1)S(1)} copy-done((bf16[1,256,1024]{2,1,0:T(8,128)(2,1)S(1)}, bf16[1,256,1024]{2,1,0:T(8,128)(2,1)}, u32[]{:S(2)}) %copy-start) | copy-done | bytes 524312
  2.1 0.0 copy-start.3
  2.1 0.8 %copy-done.3 = f32[1,2,256,16]{2,3,1,0:T(8,128)S(1)} copy-done((f32[1,2,256,16]{2,3,1,0:T(8,128)S(1)}, f32[1,2,256,16]{2,3,1,0:T(8,128)}, u32[]{:S(2)}) %copy-start.3) | copy-done | bytes 32792
  2.8 0.0 copy-start.5
  2.8 0.7 %copy-done.5 = f32[32,64]{1,0:T(8,128)S(1)} copy-done((f32[32,64]{1,0:T(8,128)S(1)}, f32[32,64]{1,0:T(8,128)}, u32[]{:S(2)}) %copy-start.5) | copy-done | bytes 8216
  3.5 19.8 %shard_map.82 = bf16[1,256,1024]{2,1,0:T(8,128)(2,1)S(1)} custom-call(bf16[1,256,1024]{2,1,0:T(8,128)(2,1)S(1)} %copy-done, bf16[1,256,256]{2,1,0:T(8,128)(2,1)S(1)} %copy-done.1, bf16[1,256,256]{2,1,0:T(8,128)(2,1)S(1)} %copy-done.2, f32[1,2,16,256]{3,2,1,0:T(8,128)S(1)} %bitcast.2, s32[1,2,4,16]{3,2,1,0:T(4,128)S(1)} %copy-done.6, f32[32,64]{1,0:T(8,128)S(1)} %copy-done.4, ...), custom_call_target="tpu_custom_call" | custom-call | tf_op jit(solution)/shard_map/pallas_call | solution.py:421
  23.4 0.8 %copy.10 = bf16[1,256,1024]{2,1,0:T(8,128)(2,1)} copy(bf16[1,256,1024]{2,1,0:T(8,128)(2,1)S(1)} %shard_map.82) | data formatting | bytes 1048576
  (2 shorter events, 0.0 us)
Async XLA Ops:
  0.0 0.7 %copy-start.7 = (f32[1024]{0:T(1024)S(1)}, f32[1024]{0:T(1024)}, u32[]{:S(2)}) copy-start(f32[1024]{0:T(1024)} %param.15) | copy-start | bytes 12292
  0.0 0.7 %copy-start.6 = (s32[1,2,4,16]{3,2,1,0:T(4,128)S(1)}, s32[1,2,4,16]{3,2,1,0:T(4,128)}, u32[]{:S(2)}) copy-start(s32[1,2,4,16]{3,2,1,0:T(4,128)} %list_ref.1) | copy-start | bytes 1540
  0.0 0.7 %copy-start.4 = (f32[32,64]{1,0:T(8,128)S(1)}, f32[32,64]{1,0:T(8,128)}, u32[]{:S(2)}) copy-start(f32[32,64]{1,0:T(8,128)} %pk_ref.1) | copy-start | bytes 24580
  0.0 0.9 %copy-start.1 = (bf16[1,256,256]{2,1,0:T(8,128)(2,1)S(1)}, bf16[1,256,256]{2,1,0:T(8,128)(2,1)}, u32[]{:S(2)}) copy-start(bf16[1,256,256]{2,1,0:T(8,128)(2,1)} %k_ref.1) | copy-start | bytes 393220
  0.0 1.0 %copy-start.2 = (bf16[1,256,256]{2,1,0:T(8,128)(2,1)S(1)}, bf16[1,256,256]{2,1,0:T(8,128)(2,1)}, u32[]{:S(2)}) copy-start(bf16[1,256,256]{2,1,0:T(8,128)(2,1)} %v_ref.1) | copy-start | bytes 393220
  1.0 1.0 %copy-start = (bf16[1,256,1024]{2,1,0:T(8,128)(2,1)S(1)}, bf16[1,256,1024]{2,1,0:T(8,128)(2,1)}, u32[]{:S(2)}) copy-start(bf16[1,256,1024]{2,1,0:T(8,128)(2,1)} %q_ref.1) | copy-start | bytes 1572868
  2.1 0.8 %copy-start.3 = (f32[1,2,256,16]{2,3,1,0:T(8,128)S(1)}, f32[1,2,256,16]{2,3,1,0:T(8,128)}, u32[]{:S(2)}) copy-start(f32[1,2,256,16]{2,3,1,0:T(8,128)} %param.11) | copy-start | bytes 98308
  2.8 0.7 %copy-start.5 = (f32[32,64]{1,0:T(8,128)S(1)}, f32[32,64]{1,0:T(8,128)}, u32[]{:S(2)}) copy-start(f32[32,64]{1,0:T(8,128)} %pv_ref.1) | copy-start | bytes 24580
where the time goes:
time: 24.5 us; the launch traced here: 24.2 us
  Pallas kernels  19.8 us (81%)
  local copies, waits for them, and re-layouts  3.74 us (15%)
  other arithmetic  0.55 us (2%)
    pallas_call x1, Pallas kernels, per_device(): pl.pallas_call(functools.partial(kernel, n), out_shape=jax.ShapeDtypeStru...  19.8 us
    unnamed x17, local copies, waits for them, and re-layouts  3.74 us
    mul x1, other arithmetic, rope_table(): return (jnp.cos(angle), jnp.sin(angle) * sign[None, :])  0.53 us

commit v1 on v0

v1 whole, which is shorter than its diff:
```python
import functools

import jax
import jax.numpy as jnp
import numpy as np
from jax import lax
from jax.experimental import pallas as pl
from jax.experimental.pallas import tpu as pltpu
from jax.sharding import PartitionSpec as P

DH = 64
CMP_STRIDE = 16
CMP_BLOCK = 32
SLC = 64
QB = 128
MOST = 2
THETA = 500000.0
EPS = 1e-06
NEG = -1e30
LOG2E = 1.4426950408889634
WIDE = 2 * DH
ONES = 16
MESH = pl.DeviceIdType.MESH


def rope_constants(n, length):
    half = DH // 2
    freq = THETA ** (-2.0 * (np.arange(WIDE) % half) / DH)
    within = np.arange(length)[:, None] * freq[None, :]
    start = np.arange(n)[:, None] * length * freq[None, :]
    base = np.stack([np.cos(within), np.sin(within)]).astype(np.float32)
    shift = np.stack([np.cos(start), np.sin(start)], 1).astype(np.float32)
    return base, shift


def kernel(
    n, q_hbm, k_hbm, v_hbm, gate_hbm, list_hbm, pk_hbm, pv_hbm, gain_hbm, base_hbm, shift_hbm,
    out_ref,
    q_ref, kv_ref, gate_ref, list_ref, pool_ref, gain_ref, base_ref, shift_ref,
    near, qt, kk, kkr, vt, vtr, sall, skk, svt, flag, own_bias, far_bias, tri, spread_map,
    req, reqbuf, sendk, sendv, recvk, recvv, wslot, slot_top,
    top, total, acc, stot, sacc,
    local, near_send, near_recv, req_send, req_recv, k_send, k_recv, v_send, v_recv,
    sum_send, sum_recv,
):
    me = lax.axis_index("kv")
    length = q_ref.shape[0]
    heads = q_ref.shape[1] // DH
    width = kv_ref.shape[2]
    groups = width // DH
    per_group = heads // groups
    pairs = per_group // 2
    slabs = groups // 2
    qblocks = length // QB
    per = length // SLC
    count = length // CMP_STRIDE
    size = MOST * SLC
    scale = DH ** (-0.5) * LOG2E
    f32, bf16 = jnp.float32, jnp.bfloat16

    barrier = pltpu.get_barrier_semaphore()

    @pl.when(me >= 1)
    def _():
        pl.semaphore_signal(barrier, inc=1, device_id={"kv": me - 1}, device_id_type=MESH)

        @pl.loop(me + 1, n)
        def _(r):
            pl.semaphore_signal(barrier, inc=1, device_id={"kv": r}, device_id_type=MESH)

    fetches = [
        pltpu.make_async_copy(src, dst, local.at[i])
        for i, (src, dst) in enumerate(
            (
                (k_hbm.at[0], kv_ref.at[0]),
                (v_hbm.at[0], kv_ref.at[1]),
                (list_hbm.at[0], list_ref),
                (base_hbm, base_ref),
                (shift_hbm, shift_ref),
                (q_hbm.at[0], q_ref),
                (pk_hbm, pool_ref.at[0]),
                (pv_hbm, pool_ref.at[1]),
                (gate_hbm.at[0], gate_ref),
                (gain_hbm, gain_ref),
            )
        )
    ]
    for fetch in fetches:
        fetch.start()

    def remote(src, dst, send, recv, peer):
        return pltpu.make_async_remote_copy(
            src_ref=src, dst_ref=dst, send_sem=send, recv_sem=recv,
            device_id={"kv": peer}, device_id_type=MESH,
        )

    def give_near(w, peer):
        return remote(kv_ref.at[w], near.at[w], near_send.at[w], near_recv.at[w], peer)

    def ask(s, origin):
        return remote(req.at[s], reqbuf.at[origin], req_send.at[s], req_recv.at[origin], s + 1)

    def give_k(r, s):
        return remote(sendk.at[r], recvk.at[s], k_send.at[r], k_recv.at[s], r)

    def give_v(r, s):
        return remote(sendv.at[r], recvv.at[s], v_send.at[r], v_recv.at[s], r)

    def give_sum(r, s):
        return remote(sall.at[s], sall.at[s], sum_send.at[r], sum_recv.at[s], r)

    def iota(shape, axis):
        return lax.broadcasted_iota(jnp.int32, shape, axis)

    fetches[0].wait()
    fetches[1].wait()
    pl.semaphore_wait(barrier, jnp.where(me < n - 1, 1, 0) + jnp.maximum(me - 1, 0))

    @pl.when(me < n - 1)
    def _():
        give_near(0, me + 1).start()
        give_near(1, me + 1).start()

    lanes = flag.shape[1]
    rows = qblocks * groups

    def column(x, at):
        spot = iota(x.shape, 1) == at
        picked = jnp.sum(jnp.where(spot, x.astype(f32), 0.0), 1, keepdims=True)
        return jnp.broadcast_to(picked, (x.shape[0], QB))

    fetches[2].wait()
    lists = jnp.concatenate([list_ref[b] for b in range(qblocks)], 0)
    lane = iota((rows, lanes), 1)
    member = jnp.zeros((rows, lanes), jnp.int32)
    for i in range(lists.shape[1]):
        member = jnp.where(lists[:, i : i + 1] == lane, 1, member)
    union = member[:groups]
    for b in range(1, qblocks):
        union = jnp.maximum(union, member[b * groups : (b + 1) * groups])
    union = jnp.concatenate([union] * qblocks, 0)
    inner = lane % per
    rank = jnp.zeros_like(union)
    for d in range(1, per):
        rank = rank + jnp.where(inner >= d, pltpu.roll(union, d, 1), 0)

    def first_of(x):
        found = x
        for d in range(1, per):
            found = found + pltpu.roll(x, lanes - d, 1)
        return found

    asked = []
    for j in range(MOST):
        hit = (union == 1) & (rank == j)
        asked.append(first_of(jnp.where(hit, inner, 0))[:groups])
        flag[j * rows : (j + 1) * rows, :] = first_of(jnp.where(hit, member, 0))
    asked = jnp.concatenate(asked, 0)
    low_row = iota((1, WIDE), 1) < DH

    @pl.loop(0, me)
    def _(s):
        ids = column(asked, s * per)
        for j in range(MOST):
            for p in range(slabs):
                at = j * groups + 2 * p
                req[s, j * slabs + p : j * slabs + p + 1, :] = jnp.where(
                    low_row, ids[at : at + 1], ids[at + 1 : at + 2]
                )

    @pl.loop(0, me - 1)
    def _(s):
        ask(s, me).start()

    for i in range(per):
        own_bias[i] = jnp.where(column(member, me * per + i) > 0.5, 0.0, NEG)
    tri[...] = jnp.where(iota((QB, QB), 0) <= iota((QB, QB), 1), 0.0, NEG)

    def lane_map(shape, source):
        return jnp.where(iota(shape, 0) == source(iota(shape, 1)), 1.0, 0.0).astype(bf16)

    half = DH // 2
    partner_map = lane_map((width, width), lambda c: c - c % DH + (c + half) % DH)
    wide_shape = (width, groups * WIDE)
    spread_map[...] = lane_map(wide_shape, lambda c: c // WIDE * DH + c % DH)
    spread_partner = lane_map(wide_shape, lambda c: c // WIDE * DH + (c + half) % DH)
    eye = lane_map((width, width), lambda c: c)

    def mapped(x, lanes_to):
        return jnp.dot(x, lanes_to, preferred_element_type=f32)

    def score(keys, queries):
        return lax.dot_general(
            keys, queries, (((1,), (1,)), ((), ())), preferred_element_type=f32
        )

    fetches[3].wait()
    fetches[4].wait()
    sign = jnp.where(iota((1, WIDE), 1) % DH < half, -1.0, 1.0)

    def tables(span):
        cos_in, sin_in = base_ref[0], base_ref[1]
        cos_at, sin_at = shift_ref[span, 0:1], shift_ref[span, 1:2]
        cosine = cos_in * cos_at - sin_in * sin_at
        sine = (sin_in * cos_at + cos_in * sin_at) * sign
        return cosine, sine

    low = iota((length, WIDE), 1) < DH
    cosine, sine = tables(me)
    plain = mapped(kv_ref[0], spread_map[...])
    other = mapped(kv_ref[0], spread_partner)
    for g in range(groups):
        cols = slice(g * WIDE, (g + 1) * WIDE)
        turned = plain[:, cols] * cosine + other[:, cols] * sine
        kk[g, 0] = jnp.where(low, turned, 0.0).astype(bf16)
        kk[g, 1] = jnp.where(low, 0.0, turned).astype(bf16)

    def flipped(x):
        return score(eye, x).astype(bf16)

    flip = flipped(kv_ref[1])
    for g in range(groups):
        vt[g, :DH] = flip[g * DH : (g + 1) * DH]
        vt[g, DH:] = jnp.ones((ONES, length), bf16)
        vtr[g, DH:] = jnp.ones((ONES, size), bf16)
        svt[g, DH:] = jnp.ones((ONES, n * count), bf16)

    cosine = cosine * scale
    sine = sine * scale
    fetches[5].wait()
    span_slabs = width // WIDE
    for p in range(heads // 2 // span_slabs):
        x = q_ref[:, p * width : (p + 1) * width]
        other = mapped(x, partner_map)
        for i in range(span_slabs):
            cols = slice(i * WIDE, (i + 1) * WIDE)
            qt[p * span_slabs + i] = (x[:, cols].astype(f32) * cosine + other[:, cols] * sine).astype(
                bf16
            )

    @pl.loop(0, groups, unroll=2)
    def _(g):
        both = kk[g].reshape(2 * length, WIDE)
        values = vt[g]
        for pair in range(pairs):
            raw = score(both, qt[g * pairs + pair])
            for e in range(2):
                h = g * per_group + 2 * pair + e
                weights, tops = [], []
                for b in range(qblocks):
                    cols = slice(b * QB, (b + 1) * QB)
                    parts = []
                    for i in range((b + 1) * QB // SLC):
                        x = raw[e * length + i * SLC : e * length + (i + 1) * SLC, cols]
                        if i * SLC < b * QB:
                            x = x + own_bias[i, pl.ds(b * groups + g, 1), :]
                        else:
                            x = x + tri[i * SLC - b * QB : (i + 1) * SLC - b * QB, :]
                        parts.append(x)
                    x = jnp.concatenate(parts, 0)
                    peak = jnp.max(x, 0, keepdims=True)
                    w = jnp.exp2(x - peak).astype(bf16)
                    if x.shape[0] < length:
                        w = jnp.concatenate([w, jnp.zeros((length - x.shape[0], QB), bf16)], 0)
                    weights.append(w)
                    tops.append(peak)
                found = jnp.dot(
                    values, jnp.concatenate(weights, 1), preferred_element_type=f32
                )
                top[h] = jnp.concatenate(tops, 1)
                total[h] = found[DH : DH + 1]
                acc[h] = found[:DH]

    fetches[6].wait()
    fetches[7].wait()

    def summarize(w, x, following, p):
        pool = pool_ref[w]
        pool = jnp.concatenate([pool, pool], 1)
        cols = slice(p * WIDE, (p + 1) * WIDE)
        x = x[:, cols].astype(f32)
        after = jnp.concatenate([x[CMP_STRIDE:], following[:, cols].astype(f32)], 0)
        shape = (count, CMP_STRIDE, WIDE)
        z = x.reshape(shape) * pool[None, :CMP_STRIDE] + after.reshape(shape) * pool[None, CMP_STRIDE:]
        found = jnp.sum(z, 1)
        return (found * scale if w == 0 else found).astype(bf16)

    for w in range(2):
        for p in range(slabs):
            sall[me, w, :, p * WIDE : (p + 1) * WIDE] = summarize(
                w, kv_ref[w], jnp.zeros((CMP_STRIDE, width), bf16), p
            )

    def gather(source, w_rows, dst, at):
        for j in range(MOST):
            for p in range(slabs):
                cols = slice(p * WIDE, (p + 1) * WIDE)
                pick = w_rows[j * slabs + p : j * slabs + p + 1, :]
                block = None
                for i in range(per):
                    weight = jnp.broadcast_to(jnp.where(pick == i, 1.0, 0.0), (SLC, WIDE))
                    term = source[i * SLC : (i + 1) * SLC, cols] * weight.astype(bf16)
                    block = term if block is None else block + term
                dst[at, j * SLC : (j + 1) * SLC, cols] = block

    @pl.when(me >= 1)
    def _():
        s = me - 1
        give_near(0, me).wait_recv()
        cosine, sine = tables(s)
        x = near[0]
        other = mapped(x, partner_map)
        slab = []
        for p in range(slabs):
            cols = slice(p * WIDE, (p + 1) * WIDE)
            slab.append((x[:, cols].astype(f32) * cosine + other[:, cols] * sine).astype(bf16))
        turned = jnp.concatenate(slab, 1)

        @pl.loop(0, n - 1 - me)
        def _(d):
            r = n - 1 - d
            ask(s, r).wait_recv()
            gather(turned, reqbuf[r], sendk, r)
            give_k(r, s).start()

        gather(turned, req[s], recvk, s)
        give_near(1, me).wait_recv()
        for w in range(2):
            for p in range(slabs):
                sall[s, w, :, p * WIDE : (p + 1) * WIDE] = summarize(
                    w, near[w], kv_ref[w, :CMP_STRIDE], p
                )

        @pl.loop(0, n - 1 - me)
        def _(d):
            r = n - 1 - d
            give_sum(r, s).start()
            gather(near[1], reqbuf[r], sendv, r)
            give_v(r, s).start()

        gather(near[1], req[s], recvv, s)

    low_size = iota((size, WIDE), 1) < DH

    def slot_scores(s):
        far_bias[...] = jnp.where(column(flag[...], s * per) > 0.5, 0.0, NEG)
        wide = mapped(recvk[s], spread_map[...])
        for g in range(groups):
            x = wide[:, g * WIDE : (g + 1) * WIDE]
            kkr[g, 0] = jnp.where(low_size, x, 0.0).astype(bf16)
            kkr[g, 1] = jnp.where(low_size, 0.0, x).astype(bf16)

        @pl.loop(0, groups, unroll=2)
        def _(g):
            rowed = [
                jnp.concatenate(
                    [
                        far_bias[pl.ds((j * qblocks + b) * groups + g, 1), :]
                        for b in range(qblocks)
                    ],
                    1,
                )
                for j in range(MOST)
            ]
            both = kkr[g].reshape(2 * size, WIDE)
            for pair in range(pairs):
                raw = score(both, qt[g * pairs + pair])
                for e in range(2):
                    h = g * per_group + 2 * pair + e
                    x = jnp.concatenate(
                        [
                            raw[e * size + j * SLC : e * size + (j + 1) * SLC] + rowed[j]
                            for j in range(MOST)
                        ],
                        0,
                    )
                    peak = jnp.max(x, 0, keepdims=True)
                    slot_top[s, h] = peak
                    wslot[s, h] = jnp.exp2(x - peak).astype(bf16)

    def slot_values(s):
        flip = flipped(recvv[s])
        for g in range(groups):
            vtr[g, :DH] = flip[g * DH : (g + 1) * DH]

        @pl.loop(0, groups, unroll=2)
        def _(g):
            values = vtr[g]
            for o in range(per_group):
                h = g * per_group + o
                found = jnp.dot(values, wslot[s, h], preferred_element_type=f32)
                old, fresh = top[h], slot_top[s, h]
                peak = jnp.maximum(old, fresh)
                keep, gain = jnp.exp2(old - peak), jnp.exp2(fresh - peak)
                top[h] = peak
                total[h] = total[h] * keep + found[DH : DH + 1] * gain
                acc[h] = acc[h] * keep + found[:DH] * gain

    @pl.when(me >= 1)
    def _():
        slot_scores(me - 1)
        slot_values(me - 1)

    @pl.loop(0, me - 1)
    def _(s):
        give_k(me, s).wait_recv()
        slot_scores(s)

    @pl.loop(0, me - 1)
    def _(s):
        give_sum(me, s).wait_recv()

    blocks = n * count
    known = iota((blocks, width), 0) < (me + 1) * count
    sum_k = jnp.where(known, sall[:, 0].reshape(blocks, width).astype(f32), 0.0).astype(bf16)
    sum_v = jnp.where(known, sall[:, 1].reshape(blocks, width).astype(f32), 0.0).astype(bf16)
    wide = mapped(sum_k, spread_map[...])
    low_blocks = iota((blocks, WIDE), 1) < DH
    flip = flipped(sum_v)
    for g in range(groups):
        x = wide[:, g * WIDE : (g + 1) * WIDE]
        skk[g, 0] = jnp.where(low_blocks, x, 0.0).astype(bf16)
        skk[g, 1] = jnp.where(low_blocks, 0.0, x).astype(bf16)
        svt[g, :DH] = flip[g * DH : (g + 1) * DH]
    part_at = iota((blocks, length), 0)
    time_at = iota((blocks, length), 1) + me * length
    sbias = jnp.where(part_at * CMP_STRIDE + CMP_BLOCK - 1 <= time_at, 0.0, NEG)
    for g in range(groups):
        both = skk[g].reshape(2 * blocks, WIDE)
        for pair in range(pairs):
            at = g * pairs + pair
            raw = score(both, q_ref[:, at * WIDE : (at + 1) * WIDE])
            for e in range(2):
                x = raw[e * blocks : (e + 1) * blocks] + sbias
                peak = jnp.maximum(jnp.max(x, 0, keepdims=True), 0.1 * NEG)
                w = jnp.exp2(x - peak).astype(bf16)
                found = jnp.dot(svt[g], w, preferred_element_type=f32)
                h = g * per_group + 2 * pair + e
                stot[h] = found[DH : DH + 1]
                sacc[h] = found[:DH]

    @pl.loop(0, me - 1)
    def _(s):
        give_v(me, s).wait_recv()
        slot_values(s)

    fetches[8].wait()
    fetches[9].wait()
    for pair in range(heads // 2):
        both = []
        for e in range(2):
            h = 2 * pair + e
            first, second = (
                1.0 / (1.0 + jnp.exp(-gate_ref[w, h : h + 1])) for w in range(2)
            )
            mixed = sacc[h] * (first / jnp.maximum(stot[h], 1.0)) + acc[h] * (
                second / total[h]
            )
            mean = jnp.sum(mixed * mixed, 0, keepdims=True) * (1.0 / DH)
            both.append(mixed * lax.rsqrt(mean + EPS))
        cols = slice(pair * WIDE, (pair + 1) * WIDE)
        flat = jnp.concatenate(both, 0).T
        out_ref[0, :, cols] = (flat * gain_ref[:, cols]).astype(bf16)

    @pl.when(me < n - 1)
    def _():
        give_near(0, me + 1).wait_send()
        give_near(1, me + 1).wait_send()

    @pl.loop(0, me - 1)
    def _(s):
        ask(s, me).wait_send()

    @pl.when(me >= 1)
    def _():
        @pl.loop(me + 1, n)
        def _(r):
            give_k(r, me - 1).wait_send()
            give_v(r, me - 1).wait_send()
            give_sum(r, me - 1).wait_send()


def per_device(queries, keys, values, gate_logits, chosen, pool_k, pool_v, out_gain):
    n = lax.axis_size("kv")
    length = queries.shape[1]
    groups = keys.shape[2] // DH
    heads = queries.shape[2] // DH
    qblocks = length // QB
    per = length // SLC
    count = length // CMP_STRIDE
    lanes = -(-n * per // 128) * 128
    rows = qblocks * groups
    width = groups * DH
    size = MOST * SLC
    slabs = groups // 2
    asked = -(-MOST * slabs // 8) * 8
    gates = gate_logits.transpose(0, 1, 3, 2)
    base, shift = rope_constants(n, length)
    bf16, f32, i32 = jnp.bfloat16, jnp.float32, jnp.int32
    vm, dma = pltpu.VMEM, pltpu.SemaphoreType.DMA
    scratch = [
        vm((length, heads * DH), bf16),
        vm((2, length, width), bf16),
        vm((2, heads, length), f32),
        vm(chosen.shape[1:], i32),
        vm((2, CMP_BLOCK, DH), f32),
        vm((1, heads * DH), f32),
        vm(base.shape, f32),
        vm(shift.shape, f32),
        vm((2, length, width), bf16),
        vm((heads // 2, length, WIDE), bf16),
        vm((groups, 2, length, WIDE), bf16),
        vm((groups, 2, size, WIDE), bf16),
        vm((groups, DH + ONES, length), bf16),
        vm((groups, DH + ONES, size), bf16),
        vm((n, 2, count, width), bf16),
        vm((groups, 2, n * count, WIDE), bf16),
        vm((groups, DH + ONES, n * count), bf16),
        vm((MOST * rows, lanes), i32),
        vm((per, rows, QB), f32),
        vm((MOST * rows, QB), f32),
        vm((QB, QB), f32),
        vm((width, groups * WIDE), bf16),
        vm((n, asked, WIDE), f32),
        vm((n, asked, WIDE), f32),
        vm((n, size, width), bf16),
        vm((n, size, width), bf16),
        vm((n, size, width), bf16),
        vm((n, size, width), bf16),
        vm((n, heads, size, length), bf16),
        vm((n, heads, 1, length), f32),
        vm((heads, 1, length), f32),
        vm((heads, 1, length), f32),
        vm((heads, DH, length), f32),
        vm((heads, 1, length), f32),
        vm((heads, DH, length), f32),
        dma((10,)), dma((2,)), dma((2,)),
        dma((n,)), dma((n,)), dma((n,)), dma((n,)), dma((n,)), dma((n,)), dma((n,)), dma((n,)),
    ]
    operands = (queries, keys, values, gates, chosen, pool_k, pool_v, out_gain[None], base, shift)
    return pl.pallas_call(
        functools.partial(kernel, n),
        out_shape=jax.ShapeDtypeStruct(queries.shape, bf16),
        in_specs=[pl.BlockSpec(memory_space=pltpu.HBM)] * 10,
        out_specs=pl.BlockSpec(memory_space=pltpu.VMEM),
        scratch_shapes=scratch,
        compiler_params=pltpu.CompilerParams(
            collective_id=0, has_side_effects=True, vmem_limit_bytes=44 << 20
        ),
    )(*(pltpu.with_memory_space_constraint(x, pltpu.HBM) for x in operands))


def solution(mesh):
    in_specs = (
        P(("grp", "dp"), "kv", "tp"),
        P(("grp", "dp"), "kv", "tp"),
        P(("grp", "dp"), "kv", "tp"),
        P(("grp", "dp"), None, "kv", "tp"),
        P(("grp", "dp"), "kv", "tp", None),
        P(),
        P(),
        P("tp"),
    )
    out_specs = P(("grp", "dp"), "kv", "tp")
    return jax.shard_map(
        per_device, mesh=mesh, in_specs=in_specs, out_specs=out_specs, check_vma=False
    )
```

time: 24.5 us -> 19.1 us (0.78)
  local copies, waits for them, and re-layouts: 3.74 us -> 0.8 us
  Pallas kernels: 19.8 us -> 18.1 us
  other arithmetic: 0.55 us -> 0 us
    unnamed x17 -> x1, local copies, waits for them, and re-layouts: 3.74 us -> 0.8 us
    pallas_call x1, Pallas kernels: 19.8 us -> 18.1 us  [per_device(): pl.pallas_call(functools.partial(kernel, n), out_shape=jax.ShapeDtypeStru...]
    mul x1 -> x0, other arithmetic: 0.53 us -> none  [rope_table(): return (jnp.cos(angle), jnp.sin(angle) * sign[None, :])]
where the time goes in v1:
time: 19.1 us; the launch traced here: 18.9 us
  Pallas kernels  18.1 us (95%)
  local copies, waits for them, and re-layouts  0.8 us (4%)
    pallas_call x1, Pallas kernels, per_device(): pl.pallas_call(functools.partial(kernel, n), out_shape=jax.ShapeDtypeStru...  18.1 us
    unnamed x1, local copies, waits for them, and re-layouts  0.8 us

profile of v1, /device:TPU:24, one launch (start us, length us, event | category | flops | bytes accessed | tf_op | source)
XLA Modules:
  0.0 18.9 jit_solution(7307816018029669953)
XLA Ops:
  0.0 18.1 %shard_map.100 = bf16[1,256,1024]{2,1,0:T(8,128)(2,1)S(1)} custom-call(bf16[1,256,1024]{2,1,0:T(8,128)(2,1)} %q_hbm.1, bf16[1,256,256]{2,1,0:T(8,128)(2,1)} %k_hbm.1, bf16[1,256,256]{2,1,0:T(8,128)(2,1)} %v_hbm.1, f32[1,2,16,256]{3,2,1,0:T(8,128)} %bitcast.2, s32[1,2,4,16]{3,2,1,0:T(4,128)} %list_hbm.1, f32[32,64]{1,0:T(8,128)} %pk_hbm.1, f32[32,64]{1,0:T(8,128)} %pv_hbm.1, ...), custom_call_target="tpu_custom_call" | custom-call | tf_op jit(solution)/shard_map/pallas_call | solution.py:541
  18.1 0.8 %copy.12 = bf16[1,256,1024]{2,1,0:T(8,128)(2,1)} copy(bf16[1,256,1024]{2,1,0:T(8,128)(2,1)S(1)} %shard_map.100) | data formatting | bytes 1048576

commit v2 on v1

--- a/solution.py
+++ b/solution.py
@@ -37,11 +37,11 @@
     n, q_hbm, k_hbm, v_hbm, gate_hbm, list_hbm, pk_hbm, pv_hbm, gain_hbm, base_hbm, shift_hbm,
     out_ref,
     q_ref, kv_ref, gate_ref, list_ref, pool_ref, gain_ref, base_ref, shift_ref,
-    near, qt, kk, kkr, vt, vtr, sall, skk, svt, flag, own_bias, far_bias, tri, spread_map,
-    req, reqbuf, sendk, sendv, recvk, recvv, wslot, slot_top,
+    near, qraw, qt, kt, vt, sall, sks, svt, wsum, flag, own_bias, far_bias, tri,
+    req, reqbuf, reqlast, edge, lastsum, sendk, sendv, recvk, recvv, wslot, slot_top,
     top, total, acc, stot, sacc,
     local, near_send, near_recv, req_send, req_recv, k_send, k_recv, v_send, v_recv,
-    sum_send, sum_recv,
+    sum_send, sum_recv, last_send, last_recv,
 ):
     me = lax.axis_index("kv")
     length = q_ref.shape[0]
@@ -106,6 +106,20 @@
     def give_v(r, s):
         return remote(sendv.at[r], recvv.at[s], v_send.at[r], v_recv.at[s], r)
 
+    def ask_last():
+        return remote(req.at[n - 2], reqlast, last_send.at[0], last_recv.at[0], n - 2)
+
+    def give_edge():
+        return remote(
+            kv_ref.at[1, pl.ds(0, CMP_STRIDE)], edge, last_send.at[1], last_recv.at[1], n - 2
+        )
+
+    def give_last_sum():
+        return remote(lastsum, sall.at[n - 2, 1], last_send.at[2], last_recv.at[2], n - 1)
+
+    def give_last_v():
+        return remote(sendv.at[0], recvv.at[n - 2], v_send.at[0], v_recv.at[n - 2], n - 1)
+
     def give_sum(r, s):
         return remote(sall.at[s], sall.at[s], sum_send.at[r], sum_recv.at[s], r)
 
@@ -116,10 +130,19 @@
     fetches[1].wait()
     pl.semaphore_wait(barrier, jnp.where(me < n - 1, 1, 0) + jnp.maximum(me - 1, 0))
 
-    @pl.when(me < n - 1)
+    last = n - 1
+
+    @pl.when(me < last)
     def _():
         give_near(0, me + 1).start()
+
+    @pl.when(me < last - 1)
+    def _():
         give_near(1, me + 1).start()
+
+    @pl.when(me == last)
+    def _():
+        give_edge().start()
 
     lanes = flag.shape[1]
     rows = qblocks * groups
@@ -167,24 +190,40 @@
                 req[s, j * slabs + p : j * slabs + p + 1, :] = jnp.where(
                     low_row, ids[at : at + 1], ids[at + 1 : at + 2]
                 )
+        for g in range(groups):
+            at = MOST * slabs + g
+            req[s, at : at + 1, :] = jnp.where(
+                low_row, ids[g : g + 1], ids[groups + g : groups + g + 1]
+            )
 
     @pl.loop(0, me - 1)
     def _(s):
         ask(s, me).start()
 
+    @pl.when(me == last)
+    def _():
+        ask_last().start()
+
     for i in range(per):
         own_bias[i] = jnp.where(column(member, me * per + i) > 0.5, 0.0, NEG)
     tri[...] = jnp.where(iota((QB, QB), 0) <= iota((QB, QB), 1), 0.0, NEG)
 
     def lane_map(shape, source):
-        return jnp.where(iota(shape, 0) == source(iota(shape, 1)), 1.0, 0.0).astype(bf16)
+        wanted = source(iota((1, shape[1]), 1))
+        return jnp.where(iota(shape, 0) == wanted, 1.0, 0.0).astype(bf16)
 
     half = DH // 2
     partner_map = lane_map((width, width), lambda c: c - c % DH + (c + half) % DH)
-    wide_shape = (width, groups * WIDE)
-    spread_map[...] = lane_map(wide_shape, lambda c: c // WIDE * DH + c % DH)
-    spread_partner = lane_map(wide_shape, lambda c: c // WIDE * DH + (c + half) % DH)
     eye = lane_map((width, width), lambda c: c)
+
+    def spread_map(side, turn):
+        shape = (per_group * DH, per_group * WIDE)
+        return lane_map(
+            shape,
+            lambda c: jnp.where(
+                c % WIDE // DH == side, c // WIDE * DH + (c + turn) % DH, -1
+            ),
+        )
 
     def mapped(x, lanes_to):
         return jnp.dot(x, lanes_to, preferred_element_type=f32)
@@ -205,15 +244,23 @@
         sine = (sin_in * cos_at + cos_in * sin_at) * sign
         return cosine, sine
 
-    low = iota((length, WIDE), 1) < DH
+    def pipelined(steps, ahead, first, second):
+        queue = [first(i) for i in range(min(ahead, steps))]
+        for i in range(steps):
+            if i + ahead < steps:
+                queue.append(first(i + ahead))
+            second(i, queue.pop(0))
+
+    def turned_slabs(x, cosine, sine):
+        other = mapped(x, partner_map)
+        found = []
+        for p in range(slabs):
+            cols = slice(p * WIDE, (p + 1) * WIDE)
+            found.append((x[:, cols].astype(f32) * cosine + other[:, cols] * sine).astype(bf16))
+        return jnp.concatenate(found, 1)
+
     cosine, sine = tables(me)
-    plain = mapped(kv_ref[0], spread_map[...])
-    other = mapped(kv_ref[0], spread_partner)
-    for g in range(groups):
-        cols = slice(g * WIDE, (g + 1) * WIDE)
-        turned = plain[:, cols] * cosine + other[:, cols] * sine
-        kk[g, 0] = jnp.where(low, turned, 0.0).astype(bf16)
-        kk[g, 1] = jnp.where(low, 0.0, turned).astype(bf16)
+    kt[...] = turned_slabs(kv_ref[0], cosine, sine)
 
     def flipped(x):
         return score(eye, x).astype(bf16)
@@ -222,54 +269,53 @@
     for g in range(groups):
         vt[g, :DH] = flip[g * DH : (g + 1) * DH]
         vt[g, DH:] = jnp.ones((ONES, length), bf16)
-        vtr[g, DH:] = jnp.ones((ONES, size), bf16)
         svt[g, DH:] = jnp.ones((ONES, n * count), bf16)
 
     cosine = cosine * scale
     sine = sine * scale
     fetches[5].wait()
-    span_slabs = width // WIDE
-    for p in range(heads // 2 // span_slabs):
-        x = q_ref[:, p * width : (p + 1) * width]
-        other = mapped(x, partner_map)
-        for i in range(span_slabs):
-            cols = slice(i * WIDE, (i + 1) * WIDE)
-            qt[p * span_slabs + i] = (x[:, cols].astype(f32) * cosine + other[:, cols] * sine).astype(
-                bf16
-            )
-
-    @pl.loop(0, groups, unroll=2)
-    def _(g):
-        both = kk[g].reshape(2 * length, WIDE)
-        values = vt[g]
-        for pair in range(pairs):
-            raw = score(both, qt[g * pairs + pair])
-            for e in range(2):
-                h = g * per_group + 2 * pair + e
-                weights, tops = [], []
-                for b in range(qblocks):
-                    cols = slice(b * QB, (b + 1) * QB)
-                    parts = []
-                    for i in range((b + 1) * QB // SLC):
-                        x = raw[e * length + i * SLC : e * length + (i + 1) * SLC, cols]
-                        if i * SLC < b * QB:
-                            x = x + own_bias[i, pl.ds(b * groups + g, 1), :]
-                        else:
-                            x = x + tri[i * SLC - b * QB : (i + 1) * SLC - b * QB, :]
-                        parts.append(x)
-                    x = jnp.concatenate(parts, 0)
-                    peak = jnp.max(x, 0, keepdims=True)
-                    w = jnp.exp2(x - peak).astype(bf16)
-                    if x.shape[0] < length:
-                        w = jnp.concatenate([w, jnp.zeros((length - x.shape[0], QB), bf16)], 0)
-                    weights.append(w)
-                    tops.append(peak)
-                found = jnp.dot(
-                    values, jnp.concatenate(weights, 1), preferred_element_type=f32
-                )
-                top[h] = jnp.concatenate(tops, 1)
-                total[h] = found[DH : DH + 1]
-                acc[h] = found[:DH]
+    spreads = [(spread_map(side, 0), spread_map(side, half)) for side in range(2)]
+    for g in range(groups):
+        x = q_ref[:, g * per_group * DH : (g + 1) * per_group * DH]
+        plain, other = (mapped(x, lanes_to) for lanes_to in spreads[g % 2])
+        for o in range(per_group):
+            cols = slice(o * WIDE, (o + 1) * WIDE)
+            qraw[g * per_group + o] = plain[:, cols].astype(bf16)
+            qt[g * per_group + o] = (plain[:, cols] * cosine + other[:, cols] * sine).astype(bf16)
+
+    def slab_of(h):
+        p = h // per_group // 2
+        return slice(p * WIDE, (p + 1) * WIDE)
+
+    def own_scores(h):
+        return score(kt[:, slab_of(h)], qt[h])
+
+    def own_values(h, raw):
+        g = h // per_group
+        weights, tops = [], []
+        for b in range(qblocks):
+            cols = slice(b * QB, (b + 1) * QB)
+            parts = []
+            for i in range((b + 1) * QB // SLC):
+                x = raw[i * SLC : (i + 1) * SLC, cols]
+                if i * SLC < b * QB:
+                    x = x + own_bias[i, b * groups + g : b * groups + g + 1, :]
+                else:
+                    x = x + tri[i * SLC - b * QB : (i + 1) * SLC - b * QB, :]
+                parts.append(x)
+            x = jnp.concatenate(parts, 0)
+            peak = jnp.max(x, 0, keepdims=True)
+            w = jnp.exp2(x - peak).astype(bf16)
+            if x.shape[0] < length:
+                w = jnp.concatenate([w, jnp.zeros((length - x.shape[0], QB), bf16)], 0)
+            weights.append(w)
+            tops.append(peak)
+        found = jnp.dot(vt[g], jnp.concatenate(weights, 1), preferred_element_type=f32)
+        top[h] = jnp.concatenate(tops, 1)
+        total[h] = found[DH : DH + 1]
+        acc[h] = found[:DH]
+
+    pipelined(heads, 6, own_scores, own_values)
 
     fetches[6].wait()
     fetches[7].wait()
@@ -303,103 +349,125 @@
                     block = term if block is None else block + term
                 dst[at, j * SLC : (j + 1) * SLC, cols] = block
 
+    def turned_values(x):
+        swapped = [x[(i ^ 1) * SLC : ((i ^ 1) + 1) * SLC] for i in range(per)]
+        return score(eye, jnp.concatenate([x, *swapped], 0)).astype(bf16)
+
+    side_row = jnp.where(low_row, 0.0, 1.0)
+
+    def gather_values(flips, w_rows, dst, at):
+        for g in range(groups):
+            span = slice(g * DH, (g + 1) * DH)
+            pick = w_rows[MOST * slabs + g : MOST * slabs + g + 1, :]
+            block = None
+            for swap in range(2):
+                for c in range(per // 2):
+                    wanted = jnp.abs(side_row - swap) + 2 * c
+                    weight = jnp.broadcast_to(jnp.where(pick == wanted, 1.0, 0.0), (DH, WIDE))
+                    start = swap * length + c * WIDE
+                    term = flips[span, start : start + WIDE] * weight.astype(bf16)
+                    block = term if block is None else block + term
+            dst[at, span, :] = block
+
+    def slot_scores(s):
+        far_bias[...] = jnp.where(column(flag[...], s * per) > 0.5, 0.0, NEG)
+
+        def first(h):
+            return score(recvk[s, :, slab_of(h)], qt[h])
+
+        def second(h, raw):
+            g = h // per_group
+            rowed = [
+                jnp.concatenate(
+                    [far_bias[(j * qblocks + b) * groups + g][None] for b in range(qblocks)], 1
+                )
+                for j in range(MOST)
+            ]
+            cut = [raw[j * SLC : (j + 1) * SLC] for j in range(MOST)]
+            peak = functools.reduce(
+                jnp.maximum,
+                [jnp.max(x, 0, keepdims=True) + row for x, row in zip(cut, rowed)],
+            )
+            peak = jnp.maximum(peak, 0.1 * NEG)
+            slot_top[s, h] = peak
+            for j in range(MOST):
+                w = jnp.exp2(cut[j] - (peak - rowed[j])).astype(bf16)
+                wslot[s, h, j * SLC : (j + 1) * SLC] = w
+
+        pipelined(heads, 6, first, second)
+
+    def slot_values(s):
+        ones = jnp.ones((ONES, size), bf16)
+
+        def first(h):
+            g = h // per_group
+            values = jnp.concatenate([recvv[s, g * DH : (g + 1) * DH, :], ones], 0)
+            return jnp.dot(values, wslot[s, h], preferred_element_type=f32)
+
+        def second(h, found):
+            old, fresh = top[h], slot_top[s, h]
+            peak = jnp.maximum(old, fresh)
+            keep, gain = jnp.exp2(old - peak), jnp.exp2(fresh - peak)
+            top[h] = peak
+            total[h] = total[h] * keep + found[DH : DH + 1] * gain
+            acc[h] = acc[h] * keep + found[:DH] * gain
+
+        pipelined(heads, 4, first, second)
+
+    @pl.when(me == last - 1)
+    def _():
+        flips = turned_values(kv_ref[1])
+        give_edge().wait_recv()
+        for p in range(slabs):
+            lastsum[:, p * WIDE : (p + 1) * WIDE] = summarize(1, kv_ref[1], edge[...], p)
+        ask_last().wait_recv()
+        gather_values(flips, reqlast, sendv, 0)
+        give_last_sum().start()
+        give_last_v().start()
+
     @pl.when(me >= 1)
     def _():
         s = me - 1
         give_near(0, me).wait_recv()
-        cosine, sine = tables(s)
-        x = near[0]
-        other = mapped(x, partner_map)
-        slab = []
-        for p in range(slabs):
-            cols = slice(p * WIDE, (p + 1) * WIDE)
-            slab.append((x[:, cols].astype(f32) * cosine + other[:, cols] * sine).astype(bf16))
-        turned = jnp.concatenate(slab, 1)
-
-        @pl.loop(0, n - 1 - me)
+        turned = turned_slabs(near[0], *tables(s))
+
+        @pl.loop(0, last - me)
         def _(d):
-            r = n - 1 - d
+            r = last - d
             ask(s, r).wait_recv()
             gather(turned, reqbuf[r], sendk, r)
             give_k(r, s).start()
 
         gather(turned, req[s], recvk, s)
-        give_near(1, me).wait_recv()
-        for w in range(2):
+        for p in range(slabs):
+            sall[s, 0, :, p * WIDE : (p + 1) * WIDE] = summarize(
+                0, near[0], kv_ref[0, :CMP_STRIDE], p
+            )
+        slot_scores(s)
+
+        @pl.when(me < last)
+        def _():
+            give_near(1, me).wait_recv()
             for p in range(slabs):
-                sall[s, w, :, p * WIDE : (p + 1) * WIDE] = summarize(
-                    w, near[w], kv_ref[w, :CMP_STRIDE], p
+                sall[s, 1, :, p * WIDE : (p + 1) * WIDE] = summarize(
+                    1, near[1], kv_ref[1, :CMP_STRIDE], p
                 )
-
-        @pl.loop(0, n - 1 - me)
-        def _(d):
-            r = n - 1 - d
-            give_sum(r, s).start()
-            gather(near[1], reqbuf[r], sendv, r)
-            give_v(r, s).start()
-
-        gather(near[1], req[s], recvv, s)
-
-    low_size = iota((size, WIDE), 1) < DH
-
-    def slot_scores(s):
-        far_bias[...] = jnp.where(column(flag[...], s * per) > 0.5, 0.0, NEG)
-        wide = mapped(recvk[s], spread_map[...])
-        for g in range(groups):
-            x = wide[:, g * WIDE : (g + 1) * WIDE]
-            kkr[g, 0] = jnp.where(low_size, x, 0.0).astype(bf16)
-            kkr[g, 1] = jnp.where(low_size, 0.0, x).astype(bf16)
-
-        @pl.loop(0, groups, unroll=2)
-        def _(g):
-            rowed = [
-                jnp.concatenate(
-                    [
-                        far_bias[pl.ds((j * qblocks + b) * groups + g, 1), :]
-                        for b in range(qblocks)
-                    ],
-                    1,
-                )
-                for j in range(MOST)
-            ]
-            both = kkr[g].reshape(2 * size, WIDE)
-            for pair in range(pairs):
-                raw = score(both, qt[g * pairs + pair])
-                for e in range(2):
-                    h = g * per_group + 2 * pair + e
-                    x = jnp.concatenate(
-                        [
-                            raw[e * size + j * SLC : e * size + (j + 1) * SLC] + rowed[j]
-                            for j in range(MOST)
-                        ],
-                        0,
-                    )
-                    peak = jnp.max(x, 0, keepdims=True)
-                    slot_top[s, h] = peak
-                    wslot[s, h] = jnp.exp2(x - peak).astype(bf16)
-
-    def slot_values(s):
-        flip = flipped(recvv[s])
-        for g in range(groups):
-            vtr[g, :DH] = flip[g * DH : (g + 1) * DH]
-
-        @pl.loop(0, groups, unroll=2)
-        def _(g):
-            values = vtr[g]
-            for o in range(per_group):
-                h = g * per_group + o
-                found = jnp.dot(values, wslot[s, h], preferred_element_type=f32)
-                old, fresh = top[h], slot_top[s, h]
-                peak = jnp.maximum(old, fresh)
-                keep, gain = jnp.exp2(old - peak), jnp.exp2(fresh - peak)
-                top[h] = peak
-                total[h] = total[h] * keep + found[DH : DH + 1] * gain
-                acc[h] = acc[h] * keep + found[:DH] * gain
-
-    @pl.when(me >= 1)
-    def _():
-        slot_scores(me - 1)
-        slot_values(me - 1)
+            flips = turned_values(near[1])
+
+            @pl.loop(0, last - me)
+            def _(d):
+                r = last - d
+                give_sum(r, s).start()
+                gather_values(flips, reqbuf[r], sendv, r)
+                give_v(r, s).start()
+
+            gather_values(flips, req[s], recvv, s)
+
+        @pl.when(me == last)
+        def _():
+            give_last_v().wait_recv()
+
+        slot_values(s)
 
     @pl.loop(0, me - 1)
     def _(s):
@@ -410,34 +478,41 @@
     def _(s):
         give_sum(me, s).wait_recv()
 
+    @pl.when(me == last)
+    def _():
+        give_last_sum().wait_recv()
+
     blocks = n * count
     known = iota((blocks, width), 0) < (me + 1) * count
     sum_k = jnp.where(known, sall[:, 0].reshape(blocks, width).astype(f32), 0.0).astype(bf16)
     sum_v = jnp.where(known, sall[:, 1].reshape(blocks, width).astype(f32), 0.0).astype(bf16)
-    wide = mapped(sum_k, spread_map[...])
-    low_blocks = iota((blocks, WIDE), 1) < DH
     flip = flipped(sum_v)
     for g in range(groups):
-        x = wide[:, g * WIDE : (g + 1) * WIDE]
-        skk[g, 0] = jnp.where(low_blocks, x, 0.0).astype(bf16)
-        skk[g, 1] = jnp.where(low_blocks, 0.0, x).astype(bf16)
         svt[g, :DH] = flip[g * DH : (g + 1) * DH]
     part_at = iota((blocks, length), 0)
     time_at = iota((blocks, length), 1) + me * length
     sbias = jnp.where(part_at * CMP_STRIDE + CMP_BLOCK - 1 <= time_at, 0.0, NEG)
-    for g in range(groups):
-        both = skk[g].reshape(2 * blocks, WIDE)
-        for pair in range(pairs):
-            at = g * pairs + pair
-            raw = score(both, q_ref[:, at * WIDE : (at + 1) * WIDE])
-            for e in range(2):
-                x = raw[e * blocks : (e + 1) * blocks] + sbias
-                peak = jnp.maximum(jnp.max(x, 0, keepdims=True), 0.1 * NEG)
-                w = jnp.exp2(x - peak).astype(bf16)
-                found = jnp.dot(svt[g], w, preferred_element_type=f32)
-                h = g * per_group + 2 * pair + e
-                stot[h] = found[DH : DH + 1]
-                sacc[h] = found[:DH]
+
+    sks[...] = sum_k
+
+    def summary_scores(h):
+        return score(sks[:, slab_of(h)], qraw[h])
+
+    def summary_weights(h, raw):
+        x = raw + sbias
+        peak = jnp.maximum(jnp.max(x, 0, keepdims=True), 0.1 * NEG)
+        wsum[h] = jnp.exp2(x - peak).astype(bf16)
+
+    pipelined(heads, 6, summary_scores, summary_weights)
+
+    def summary_values(h):
+        return jnp.dot(svt[h // per_group], wsum[h], preferred_element_type=f32)
+
+    def summary_out(h, found):
+        stot[h] = found[DH : DH + 1]
+        sacc[h] = found[:DH]
+
+    pipelined(heads, 4, summary_values, summary_out)
 
     @pl.loop(0, me - 1)
     def _(s):
@@ -462,10 +537,23 @@
         flat = jnp.concatenate(both, 0).T
         out_ref[0, :, cols] = (flat * gain_ref[:, cols]).astype(bf16)
 
-    @pl.when(me < n - 1)
+    @pl.when(me < last)
     def _():
         give_near(0, me + 1).wait_send()
+
+    @pl.when(me < last - 1)
+    def _():
         give_near(1, me + 1).wait_send()
+
+    @pl.when(me == last - 1)
+    def _():
+        give_last_sum().wait_send()
+        give_last_v().wait_send()
+
+    @pl.when(me == last)
+    def _():
+        give_edge().wait_send()
+        ask_last().wait_send()
 
     @pl.loop(0, me - 1)
     def _(s):
@@ -493,7 +581,7 @@
     width = groups * DH
     size = MOST * SLC
     slabs = groups // 2
-    asked = -(-MOST * slabs // 8) * 8
+    asked = -(-(MOST * slabs + groups) // 8) * 8
     gates = gate_logits.transpose(0, 1, 3, 2)
     base, shift = rope_constants(n, length)
     bf16, f32, i32 = jnp.bfloat16, jnp.float32, jnp.int32
@@ -508,25 +596,27 @@
         vm(base.shape, f32),
         vm(shift.shape, f32),
         vm((2, length, width), bf16),
-        vm((heads // 2, length, WIDE), bf16),
-        vm((groups, 2, length, WIDE), bf16),
-        vm((groups, 2, size, WIDE), bf16),
+        vm((heads, length, WIDE), bf16),
+        vm((heads, length, WIDE), bf16),
+        vm((length, width), bf16),
         vm((groups, DH + ONES, length), bf16),
-        vm((groups, DH + ONES, size), bf16),
         vm((n, 2, count, width), bf16),
-        vm((groups, 2, n * count, WIDE), bf16),
+        vm((n * count, width), bf16),
         vm((groups, DH + ONES, n * count), bf16),
+        vm((heads, n * count, length), bf16),
         vm((MOST * rows, lanes), i32),
         vm((per, rows, QB), f32),
         vm((MOST * rows, QB), f32),
         vm((QB, QB), f32),
-        vm((width, groups * WIDE), bf16),
         vm((n, asked, WIDE), f32),
         vm((n, asked, WIDE), f32),
+        vm((asked, WIDE), f32),
+        vm((CMP_STRIDE, width), bf16),
+        vm((count, width), bf16),
         vm((n, size, width), bf16),
+        vm((n, width, size), bf16),
         vm((n, size, width), bf16),
-        vm((n, size, width), bf16),
-        vm((n, size, width), bf16),
+        vm((n, width, size), bf16),
         vm((n, heads, size, length), bf16),
         vm((n, heads, 1, length), f32),
         vm((heads, 1, length), f32),
@@ -536,6 +626,7 @@
         vm((heads, DH, length), f32),
         dma((10,)), dma((2,)), dma((2,)),
         dma((n,)), dma((n,)), dma((n,)), dma((n,)), dma((n,)), dma((n,)), dma((n,)), dma((n,)),
+        dma((3,)), dma((3,)),
     ]
     operands = (queries, keys, values, gates, chosen, pool_k, pool_v, out_gain[None], base, shift)
     return pl.pallas_call(

time: 19.1 us -> 16.6 us (0.87)
  the two profiles are of different devices: /device:TPU:24 before, /device:TPU:20 now
where the time goes in v2:
time: 16.6 us; the launch traced here: 16.4 us
  Pallas kernels  15.6 us (94%)
  local copies, waits for them, and re-layouts  0.8 us (5%)
    pallas_call x1, Pallas kernels, per_device(): pl.pallas_call(functools.partial(kernel, n), out_shape=jax.ShapeDtypeStru...  15.6 us
    unnamed x1, local copies, waits for them, and re-layouts  0.8 us

profile of v2, /device:TPU:20, one launch (start us, length us, event | category | flops | bytes accessed | tf_op | source)
XLA Modules:
  0.0 16.4 jit_solution(3226323016564880711)
XLA Ops:
  0.0 15.6 %shard_map.100 = bf16[1,256,1024]{2,1,0:T(8,128)(2,1)S(1)} custom-call(bf16[1,256,1024]{2,1,0:T(8,128)(2,1)} %q_hbm.1, bf16[1,256,256]{2,1,0:T(8,128)(2,1)} %k_hbm.1, bf16[1,256,256]{2,1,0:T(8,128)(2,1)} %v_hbm.1, f32[1,2,16,256]{3,2,1,0:T(8,128)} %bitcast.2, s32[1,2,4,16]{3,2,1,0:T(4,128)} %list_hbm.1, f32[32,64]{1,0:T(8,128)} %pk_hbm.1, f32[32,64]{1,0:T(8,128)} %pv_hbm.1, ...), custom_call_target="tpu_custom_call" | custom-call | tf_op jit(solution)/shard_map/pallas_call | solution.py:632
  15.6 0.8 %copy.12 = bf16[1,256,1024]{2,1,0:T(8,128)(2,1)} copy(bf16[1,256,1024]{2,1,0:T(8,128)(2,1)S(1)} %shard_map.100) | data formatting | bytes 1048576

commit v3 on v2

--- a/solution.py
+++ b/solution.py
@@ -38,7 +38,7 @@
     out_ref,
     q_ref, kv_ref, gate_ref, list_ref, pool_ref, gain_ref, base_ref, shift_ref,
     near, qraw, qt, kt, vt, sall, sks, svt, wsum, flag, own_bias, far_bias, tri,
-    req, reqbuf, reqlast, edge, lastsum, sendk, sendv, recvk, recvv, wslot, slot_top,
+    req, reqbuf, reqlast, edge, lastsum, sendk, sendv, recvk, recvv, wslot, slot_top, slot_total, gain_at,
     top, total, acc, stot, sacc,
     local, near_send, near_recv, req_send, req_recv, k_send, k_recv, v_send, v_recv,
     sum_send, sum_recv, last_send, last_recv,
@@ -311,11 +311,16 @@
             weights.append(w)
             tops.append(peak)
         found = jnp.dot(vt[g], jnp.concatenate(weights, 1), preferred_element_type=f32)
-        top[h] = jnp.concatenate(tops, 1)
-        total[h] = found[DH : DH + 1]
+        top[h : h + 1] = jnp.concatenate(tops, 1)
+        total[h : h + 1] = found[DH : DH + 1]
         acc[h] = found[:DH]
 
     pipelined(heads, 6, own_scores, own_values)
+
+    fetches[9].wait()
+    for pair in range(heads // 2):
+        row = gain_ref[:, pair * WIDE : (pair + 1) * WIDE]
+        gain_at[pair] = jnp.broadcast_to(row, (WIDE, WIDE)).T
 
     fetches[6].wait()
     fetches[7].wait()
@@ -389,30 +394,33 @@
                 [jnp.max(x, 0, keepdims=True) + row for x, row in zip(cut, rowed)],
             )
             peak = jnp.maximum(peak, 0.1 * NEG)
-            slot_top[s, h] = peak
+            slot_top[s, h : h + 1] = peak
+            sums = []
             for j in range(MOST):
-                w = jnp.exp2(cut[j] - (peak - rowed[j])).astype(bf16)
-                wslot[s, h, j * SLC : (j + 1) * SLC] = w
+                w = jnp.exp2(cut[j] - (peak - rowed[j]))
+                sums.append(jnp.sum(w, 0, keepdims=True))
+                wslot[s, h, j * SLC : (j + 1) * SLC] = w.astype(bf16)
+            slot_total[s, h : h + 1] = functools.reduce(jnp.add, sums)
 
         pipelined(heads, 6, first, second)
 
+    def slot_product(s, h):
+        g = h // per_group
+        return jnp.dot(
+            recvv[s, g * DH : (g + 1) * DH, :], wslot[s, h], preferred_element_type=f32
+        )
+
     def slot_values(s):
-        ones = jnp.ones((ONES, size), bf16)
-
-        def first(h):
-            g = h // per_group
-            values = jnp.concatenate([recvv[s, g * DH : (g + 1) * DH, :], ones], 0)
-            return jnp.dot(values, wslot[s, h], preferred_element_type=f32)
+        old, fresh = top[...], slot_top[s]
+        peak = jnp.maximum(old, fresh)
+        keep, gain = jnp.exp2(old - peak), jnp.exp2(fresh - peak)
+        top[...] = peak
+        total[...] = total[...] * keep + slot_total[s] * gain
 
         def second(h, found):
-            old, fresh = top[h], slot_top[s, h]
-            peak = jnp.maximum(old, fresh)
-            keep, gain = jnp.exp2(old - peak), jnp.exp2(fresh - peak)
-            top[h] = peak
-            total[h] = total[h] * keep + found[DH : DH + 1] * gain
-            acc[h] = acc[h] * keep + found[:DH] * gain
-
-        pipelined(heads, 4, first, second)
+            acc[h] = acc[h] * keep[h : h + 1] + found * gain[h : h + 1]
+
+        pipelined(heads, 4, lambda h: slot_product(s, h), second)
 
     @pl.when(me == last - 1)
     def _():
@@ -452,12 +460,16 @@
                 sall[s, 1, :, p * WIDE : (p + 1) * WIDE] = summarize(
                     1, near[1], kv_ref[1, :CMP_STRIDE], p
                 )
+
+            @pl.loop(me + 1, n)
+            def _(r):
+                give_sum(r, s).start()
+
             flips = turned_values(near[1])
 
             @pl.loop(0, last - me)
             def _(d):
                 r = last - d
-                give_sum(r, s).start()
                 gather_values(flips, reqbuf[r], sendv, r)
                 give_v(r, s).start()
 
@@ -509,33 +521,50 @@
         return jnp.dot(svt[h // per_group], wsum[h], preferred_element_type=f32)
 
     def summary_out(h, found):
-        stot[h] = found[DH : DH + 1]
+        stot[h : h + 1] = found[DH : DH + 1]
         sacc[h] = found[:DH]
 
     pipelined(heads, 4, summary_values, summary_out)
+
+    fetches[8].wait()
+    first_gate, second_gate = (1.0 / (1.0 + jnp.exp(-gate_ref[w])) for w in range(2))
+    far = jnp.maximum(me - 1, 0)
+    peak = lax.fori_loop(0, far, lambda s, x: jnp.maximum(x, slot_top[s]), top[...])
+    keep = jnp.exp2(top[...] - peak)
+    whole = lax.fori_loop(
+        0,
+        far,
+        lambda s, x: x + slot_total[s] * jnp.exp2(slot_top[s] - peak),
+        total[...] * keep,
+    )
+    shared = second_gate / whole
+    keep = keep * shared
+    first_gate = first_gate / jnp.maximum(stot[...], 1.0)
+
+    @pl.loop(0, me - 1)
+    def _(s):
+        slot_top[s] = jnp.exp2(slot_top[s] - peak) * shared
+
+    for h in range(heads):
+        acc[h] = sacc[h] * first_gate[h : h + 1] + acc[h] * keep[h : h + 1]
 
     @pl.loop(0, me - 1)
     def _(s):
         give_v(me, s).wait_recv()
-        slot_values(s)
-
-    fetches[8].wait()
-    fetches[9].wait()
+
+        def second(h, found):
+            acc[h] = acc[h] + found * slot_top[s, h : h + 1]
+
+        pipelined(heads, 4, lambda h: slot_product(s, h), second)
+
     for pair in range(heads // 2):
         both = []
         for e in range(2):
-            h = 2 * pair + e
-            first, second = (
-                1.0 / (1.0 + jnp.exp(-gate_ref[w, h : h + 1])) for w in range(2)
-            )
-            mixed = sacc[h] * (first / jnp.maximum(stot[h], 1.0)) + acc[h] * (
-                second / total[h]
-            )
+            mixed = acc[2 * pair + e]
             mean = jnp.sum(mixed * mixed, 0, keepdims=True) * (1.0 / DH)
             both.append(mixed * lax.rsqrt(mean + EPS))
-        cols = slice(pair * WIDE, (pair + 1) * WIDE)
-        flat = jnp.concatenate(both, 0).T
-        out_ref[0, :, cols] = (flat * gain_ref[:, cols]).astype(bf16)
+        flat = jnp.concatenate(both, 0) * jnp.concatenate([gain_at[pair]] * (length // WIDE), 1)
+        out_ref[0, :, pair * WIDE : (pair + 1) * WIDE] = flat.astype(bf16).T
 
     @pl.when(me < last)
     def _():
@@ -618,11 +647,13 @@
         vm((n, size, width), bf16),
         vm((n, width, size), bf16),
         vm((n, heads, size, length), bf16),
-        vm((n, heads, 1, length), f32),
-        vm((heads, 1, length), f32),
-        vm((heads, 1, length), f32),
+        vm((n, heads, length), f32),
+        vm((n, heads, length), f32),
+        vm((heads // 2, WIDE, WIDE), f32),
+        vm((heads, length), f32),
+        vm((heads, length), f32),
         vm((heads, DH, length), f32),
-        vm((heads, 1, length), f32),
+        vm((heads, length), f32),
         vm((heads, DH, length), f32),
         dma((10,)), dma((2,)), dma((2,)),
         dma((n,)), dma((n,)), dma((n,)), dma((n,)), dma((n,)), dma((n,)), dma((n,)), dma((n,)),

time: 16.6 us -> 16.4 us (0.988)
  the two profiles are of different devices: /device:TPU:20 before, /device:TPU:16 now
where the time goes in v3:
time: 16.4 us; the launch traced here: 16.3 us
  Pallas kernels  15.5 us (95%)
  local copies, waits for them, and re-layouts  0.8 us (5%)
    pallas_call x1, Pallas kernels, per_device(): pl.pallas_call(functools.partial(kernel, n), out_shape=jax.ShapeDtypeStru...  15.5 us
    unnamed x1, local copies, waits for them, and re-layouts  0.8 us

profile of v3, /device:TPU:16, one launch (start us, length us, event | category | flops | bytes accessed | tf_op | source)
XLA Modules:
  0.0 16.3 jit_solution(3618254949921442588)
XLA Ops:
  0.0 15.5 %shard_map.100 = bf16[1,256,1024]{2,1,0:T(8,128)(2,1)S(1)} custom-call(bf16[1,256,1024]{2,1,0:T(8,128)(2,1)} %q_hbm.1, bf16[1,256,256]{2,1,0:T(8,128)(2,1)} %k_hbm.1, bf16[1,256,256]{2,1,0:T(8,128)(2,1)} %v_hbm.1, f32[1,2,16,256]{3,2,1,0:T(8,128)} %bitcast.2, s32[1,2,4,16]{3,2,1,0:T(4,128)} %list_hbm.1, f32[32,64]{1,0:T(8,128)} %pk_hbm.1, f32[32,64]{1,0:T(8,128)} %pv_hbm.1, ...), custom_call_target="tpu_custom_call" | custom-call | tf_op jit(solution)/shard_map/pallas_call | solution.py:663
  15.5 0.8 %copy.12 = bf16[1,256,1024]{2,1,0:T(8,128)(2,1)} copy(bf16[1,256,1024]{2,1,0:T(8,128)(2,1)S(1)} %shard_map.100) | data formatting | bytes 1048576

commit v4 on v3

--- a/solution.py
+++ b/solution.py
@@ -467,19 +467,13 @@
 
             flips = turned_values(near[1])
 
-            @pl.loop(0, last - me)
-            def _(d):
-                r = last - d
+            @pl.loop(me + 1, n)
+            def _(r):
                 gather_values(flips, reqbuf[r], sendv, r)
                 give_v(r, s).start()
 
             gather_values(flips, req[s], recvv, s)
-
-        @pl.when(me == last)
-        def _():
-            give_last_v().wait_recv()
-
-        slot_values(s)
+            slot_values(s)
 
     @pl.loop(0, me - 1)
     def _(s):
@@ -528,7 +522,7 @@
 
     fetches[8].wait()
     first_gate, second_gate = (1.0 / (1.0 + jnp.exp(-gate_ref[w])) for w in range(2))
-    far = jnp.maximum(me - 1, 0)
+    far = jnp.where(me == last, me, jnp.maximum(me - 1, 0))
     peak = lax.fori_loop(0, far, lambda s, x: jnp.maximum(x, slot_top[s]), top[...])
     keep = jnp.exp2(top[...] - peak)
     whole = lax.fori_loop(
@@ -541,30 +535,59 @@
     keep = keep * shared
     first_gate = first_gate / jnp.maximum(stot[...], 1.0)
 
-    @pl.loop(0, me - 1)
+    @pl.loop(0, far)
     def _(s):
         slot_top[s] = jnp.exp2(slot_top[s] - peak) * shared
 
     for h in range(heads):
         acc[h] = sacc[h] * first_gate[h : h + 1] + acc[h] * keep[h : h + 1]
 
-    @pl.loop(0, me - 1)
-    def _(s):
-        give_v(me, s).wait_recv()
-
-        def second(h, found):
-            acc[h] = acc[h] + found * slot_top[s, h : h + 1]
-
-        pipelined(heads, 4, lambda h: slot_product(s, h), second)
-
-    for pair in range(heads // 2):
+    def finish(pair, heads_mixed):
         both = []
-        for e in range(2):
-            mixed = acc[2 * pair + e]
+        for mixed in heads_mixed:
             mean = jnp.sum(mixed * mixed, 0, keepdims=True) * (1.0 / DH)
             both.append(mixed * lax.rsqrt(mean + EPS))
         flat = jnp.concatenate(both, 0) * jnp.concatenate([gain_at[pair]] * (length // WIDE), 1)
         out_ref[0, :, pair * WIDE : (pair + 1) * WIDE] = flat.astype(bf16).T
+
+    def heads_of(pair):
+        return range(2 * pair, 2 * pair + 2)
+
+    def added(s, h, found):
+        return acc[h] + found * slot_top[s, h : h + 1]
+
+    def add_slot(s):
+        def second(h, found):
+            acc[h] = added(s, h, found)
+
+        pipelined(heads, 4, lambda h: slot_product(s, h), second)
+
+    @pl.when(me == last)
+    def _():
+        give_last_v().wait_recv()
+        add_slot(me - 1)
+
+    @pl.loop(1, me - 1)
+    def _(s):
+        give_v(me, s).wait_recv()
+        add_slot(s)
+
+    @pl.when(me >= 2)
+    def _():
+        give_v(me, 0).wait_recv()
+        pipelined(
+            heads // 2,
+            4,
+            lambda pair: [slot_product(0, h) for h in heads_of(pair)],
+            lambda pair, found: finish(
+                pair, [added(0, h, x) for h, x in zip(heads_of(pair), found)]
+            ),
+        )
+
+    @pl.when(me < 2)
+    def _():
+        for pair in range(heads // 2):
+            finish(pair, [acc[h] for h in heads_of(pair)])
 
     @pl.when(me < last)
     def _():

time: 16.4 us -> 16.2 us (0.988)
  the two profiles are of different devices: /device:TPU:16 before, /device:TPU:24 now
where the time goes in v4:
time: 16.2 us; the launch traced here: 16.1 us
  Pallas kernels  15.3 us (94%)
  local copies, waits for them, and re-layouts  0.8 us (5%)
    pallas_call x1, Pallas kernels, per_device(): pl.pallas_call(functools.partial(kernel, n), out_shape=jax.ShapeDtypeStru...  15.3 us
    unnamed x1, local copies, waits for them, and re-layouts  0.8 us

profile of v4, /device:TPU:24, one launch (start us, length us, event | category | flops | bytes accessed | tf_op | source)
XLA Modules:
  0.0 16.1 jit_solution(16821280720303300536)
XLA Ops:
  0.0 15.3 %shard_map.100 = bf16[1,256,1024]{2,1,0:T(8,128)(2,1)S(1)} custom-call(bf16[1,256,1024]{2,1,0:T(8,128)(2,1)} %q_hbm.1, bf16[1,256,256]{2,1,0:T(8,128)(2,1)} %k_hbm.1, bf16[1,256,256]{2,1,0:T(8,128)(2,1)} %v_hbm.1, f32[1,2,16,256]{3,2,1,0:T(8,128)} %bitcast.2, s32[1,2,4,16]{3,2,1,0:T(4,128)} %list_hbm.1, f32[32,64]{1,0:T(8,128)} %pk_hbm.1, f32[32,64]{1,0:T(8,128)} %pv_hbm.1, ...), custom_call_target="tpu_custom_call" | custom-call | tf_op jit(solution)/shard_map/pallas_call | solution.py:686
  15.3 0.8 %copy.12 = bf16[1,256,1024]{2,1,0:T(8,128)(2,1)} copy(bf16[1,256,1024]{2,1,0:T(8,128)(2,1)S(1)} %shard_map.100) | data formatting | bytes 1048576

commit v5 on v4

--- a/solution.py
+++ b/solution.py
@@ -420,7 +420,7 @@
         def second(h, found):
             acc[h] = acc[h] * keep[h : h + 1] + found * gain[h : h + 1]
 
-        pipelined(heads, 4, lambda h: slot_product(s, h), second)
+        pipelined(heads, 8, lambda h: slot_product(s, h), second)
 
     @pl.when(me == last - 1)
     def _():
@@ -509,7 +509,7 @@
         peak = jnp.maximum(jnp.max(x, 0, keepdims=True), 0.1 * NEG)
         wsum[h] = jnp.exp2(x - peak).astype(bf16)
 
-    pipelined(heads, 6, summary_scores, summary_weights)
+    pipelined(heads, 10, summary_scores, summary_weights)
 
     def summary_values(h):
         return jnp.dot(svt[h // per_group], wsum[h], preferred_element_type=f32)
@@ -518,7 +518,7 @@
         stot[h : h + 1] = found[DH : DH + 1]
         sacc[h] = found[:DH]
 
-    pipelined(heads, 4, summary_values, summary_out)
+    pipelined(heads, 8, summary_values, summary_out)
 
     fetches[8].wait()
     first_gate, second_gate = (1.0 / (1.0 + jnp.exp(-gate_ref[w])) for w in range(2))
@@ -560,7 +560,7 @@
         def second(h, found):
             acc[h] = added(s, h, found)
 
-        pipelined(heads, 4, lambda h: slot_product(s, h), second)
+        pipelined(heads, 8, lambda h: slot_product(s, h), second)
 
     @pl.when(me == last)
     def _():

time: 16.2 us -> 16.2 us (level)
  no operation moved by 1% of the time
where the time goes in v5:
time: 16.2 us; the launch traced here: 16.1 us
  Pallas kernels  15.3 us (94%)
  local copies, waits for them, and re-layouts  0.8 us (5%)
    pallas_call x1, Pallas kernels, per_device(): pl.pallas_call(functools.partial(kernel, n), out_shape=jax.ShapeDtypeStru...  15.3 us
    unnamed x1, local copies, waits for them, and re-layouts  0.8 us

profile of v5, /device:TPU:24, one launch (start us, length us, event | category | flops | bytes accessed | tf_op | source)
XLA Modules:
  0.0 16.1 jit_solution(2321858873637729324)
XLA Ops:
  0.0 15.3 %shard_map.100 = bf16[1,256,1024]{2,1,0:T(8,128)(2,1)S(1)} custom-call(bf16[1,256,1024]{2,1,0:T(8,128)(2,1)} %q_hbm.1, bf16[1,256,256]{2,1,0:T(8,128)(2,1)} %k_hbm.1, bf16[1,256,256]{2,1,0:T(8,128)(2,1)} %v_hbm.1, f32[1,2,16,256]{3,2,1,0:T(8,128)} %bitcast.2, s32[1,2,4,16]{3,2,1,0:T(4,128)} %list_hbm.1, f32[32,64]{1,0:T(8,128)} %pk_hbm.1, f32[32,64]{1,0:T(8,128)} %pv_hbm.1, ...), custom_call_target="tpu_custom_call" | custom-call | tf_op jit(solution)/shard_map/pallas_call | solution.py:686
  15.3 0.8 %copy.12 = bf16[1,256,1024]{2,1,0:T(8,128)(2,1)} copy(bf16[1,256,1024]{2,1,0:T(8,128)(2,1)S(1)} %shard_map.100) | data formatting | bytes 1048576
